TPU v7x, 32 devices: a whole 2x2x4 slice. The times are simulated.
32 devices in a mesh: kv: 16 (over z, y, core), tp: 2 (over x).
Axes of the slice: x: 2, y: 2, z: 4, core: 2. Of those that a mesh axis runs over, the one named last changes fastest.
Arguments:
- tokens: bfloat16 [6144, 1024], P('kv', 'tp'), may hold values from -6 to 6
- query_weight: bfloat16 [1024, 512], P(None, 'tp'), may hold values from -0.1875 to 0.1875
- key_weight: bfloat16 [1024, 512], P(None, 'tp'), may hold values from -0.1875 to 0.1875
- value_weight: bfloat16 [1024, 512], P(None, 'tp'), may hold values from -0.1875 to 0.1875
- out_weight: bfloat16 [512, 1024], P('tp'), may hold values from -0.25 to 0.25
- norm_gain: float32 [512], P('tp'), may hold values from 0.1 to 1.9
- chosen_owner: int32 [96, 8], P('kv'), may hold values from 0 to 15, all different within a row; in each aligned block of 6 rows (0 to 5, 6 to 11, ...) at most 6 rows name the same one
- chosen_local: int32 [96, 8], P('kv'), may hold values from 0 to 5
Outputs:
- attended_out: bfloat16 [6144, 1024], P('kv', 'tp')
Inputs may be any that keep to these rules, and one draw needn't show every extreme that they name: `chosen_owner`: each row names 8 different owners; among the 6 rows of one device no owner is named by more than 6 rows, and in some device's rows one owner is named by exactly 6. `chosen_local`: any index of a key block within its owner.
All inputs are finite; a program needn't handle non-finite values.
Results may differ from a plain program's by a relative error of at most 0.015.
Values may be sent and summed in bfloat16 or wider, within the bound.
A program may use at most 64 MiB of HBM per device.

v0:
```python
import jax
import jax.numpy as jnp
from jax import lax
from jax.sharding import PartitionSpec as P

HEADS = 8
HEAD_SIZE = 64
BLOCK = 64


neg_fill = -1e30
eps_norm = 1e-06


def folded(value, axis, dim, take_in, carry):
    whole = jax.tree.map(lambda part: lax.all_gather(part, axis, axis=dim, tiled=True), value)
    return take_in(carry, whole, jnp.int32(0))


def for_sending(value):
    return jax.tree.map(lambda a: a.astype(jnp.bfloat16) if a.dtype == jnp.float32 else a, value)


def scattered(portion, width, axis):
    count = width * lax.axis_size(axis)
    sent = portion(jnp.int32(0), count).astype(jnp.bfloat16)
    return lax.psum_scatter(sent, axis, scatter_dimension=0, tiled=True).astype(jnp.float32)


def partial_softmax(query_rows, key_rows, value_rows, query_pos, key_pos):
    score_scale = query_rows.shape[-1] ** (-0.5)
    scores = (
        jnp.einsum("bqhd,bcthd->bhqct", query_rows, key_rows, preferred_element_type=jnp.float32)
        * score_scale
    )
    visible = key_pos[:, None, None, :, :] <= query_pos[:, None, :, None, None]
    scores = jnp.where(visible, scores, neg_fill)
    highest = jnp.max(scores, axis=(3, 4))
    weights = jnp.where(visible, jnp.exp(scores - highest[:, :, :, None, None]), jnp.float32(0.0))
    mass_sum = jnp.sum(weights, axis=(3, 4))
    blended = jnp.einsum(
        "bhqct,bcthd->bqhd",
        weights,
        value_rows.astype(jnp.float32),
        precision=lax.Precision.HIGHEST,
    )
    return (highest, mass_sum, blended)


def on_device(
    tokens,
    query_weight,
    key_weight,
    value_weight,
    out_weight,
    norm_gain,
    chosen_owner,
    chosen_local,
):
    tok_rows = tokens.shape[0]
    blocks_here = tok_rows // BLOCK
    heads_here = query_weight.shape[1] // HEAD_SIZE
    empty_sum = jnp.zeros((tok_rows, query_weight.shape[1]), jnp.float32)

    def add_columns(carried, portion, offset):
        span_rows = portion.shape[1]
        return tuple(
            (
                partial_sum
                + jnp.dot(
                    portion,
                    lax.dynamic_slice_in_dim(weight, offset, span_rows, 0),
                    preferred_element_type=jnp.float32,
                )
                for partial_sum, weight in zip(carried, (query_weight, key_weight, value_weight))
            )
        )

    projected = folded(tokens, "tp", 1, add_columns, (empty_sum, empty_sum, empty_sum))
    local_queries, local_keys, local_values = [
        summed.astype(jnp.bfloat16).reshape(blocks_here, BLOCK, heads_here, HEAD_SIZE)
        for summed in projected
    ]
    device = lax.axis_index("kv")
    kv_count = lax.axis_size("kv")
    chosen_count = chosen_owner.shape[1]
    capacity = min(blocks_here, max(1, 2 * blocks_here * chosen_count // kv_count))
    offsets = jnp.arange(BLOCK, dtype=jnp.int32)
    own_global = device * blocks_here + jnp.arange(blocks_here, dtype=jnp.int32)
    query_pos = own_global[:, None] * BLOCK + offsets[None, :]
    flat_owner = chosen_owner.reshape(-1)
    one_hot = (flat_owner[:, None] == jnp.arange(kv_count, dtype=jnp.int32)[None, :]).astype(
        jnp.int32
    )
    earlier = jnp.cumsum(one_hot, axis=0) - one_hot
    flat_slot = jnp.sum(earlier * one_hot, axis=1)
    requests = (
        jnp.zeros((kv_count, capacity), jnp.int32)
        .at[flat_owner, flat_slot]
        .set(chosen_local.reshape(-1))
    )
    incoming = lax.all_to_all(requests, "kv", split_axis=0, concat_axis=0, tiled=True)
    key_pack = local_keys[incoming]
    value_pack = local_values[incoming]
    key_back, value_back = (
        lax.all_to_all(for_sending(key_pack), "kv", split_axis=0, concat_axis=0, tiled=True).astype(
            key_pack.dtype
        ),
        lax.all_to_all(
            for_sending(value_pack), "kv", split_axis=0, concat_axis=0, tiled=True
        ).astype(value_pack.dtype),
    )
    chosen_keys = key_back[flat_owner, flat_slot].reshape(
        blocks_here, chosen_count, BLOCK, heads_here, HEAD_SIZE
    )
    chosen_values = value_back[flat_owner, flat_slot].reshape(
        blocks_here, chosen_count, BLOCK, heads_here, HEAD_SIZE
    )
    all_keys = jnp.concatenate([local_keys[:, None], chosen_keys], axis=1)
    all_values = jnp.concatenate([local_values[:, None], chosen_values], axis=1)
    own_kpos = (own_global[:, None] * BLOCK + offsets[None, :])[:, None, :]
    chosen_kpos = jnp.full((blocks_here, chosen_count, BLOCK), -1, jnp.int32)
    key_pos = jnp.concatenate([own_kpos, chosen_kpos], axis=1)
    highest, mass_sum, blended = partial_softmax(
        local_queries, all_keys, all_values, query_pos, key_pos
    )
    attended = blended / jnp.transpose(mass_sum, (0, 2, 1))[..., None]
    attended = attended.astype(jnp.bfloat16).reshape(tok_rows, heads_here * HEAD_SIZE)
    wide_rows = attended.astype(jnp.float32)
    squares = lax.psum(jnp.sum(wide_rows * wide_rows, axis=1), "tp")
    mean_sq = squares / (HEADS * HEAD_SIZE)
    normed = (wide_rows * lax.rsqrt(mean_sq + eps_norm)[:, None] * norm_gain).astype(jnp.bfloat16)
    out_cols = out_weight.shape[1] // lax.axis_size("tp")

    def out_term(offset, count):
        columns = lax.dynamic_slice_in_dim(out_weight, offset, count, 1)
        return jnp.einsum("fc,tf->ct", columns, normed, preferred_element_type=jnp.float32)

    summed = scattered(out_term, out_cols, "tp")
    return summed.T.astype(jnp.bfloat16)


def solution(mesh):
    return jax.shard_map(
        on_device,
        mesh=mesh,
        in_specs=(
            P("kv", "tp"),
            P(None, "tp"),
            P(None, "tp"),
            P(None, "tp"),
            P("tp", None),
            P("tp"),
            P("kv", None),
            P("kv", None),
        ),
        out_specs=P("kv", "tp"),
        check_vma=False,
    )
```

profile of v0, /device:TPU:0, one launch (start us, length us, event | category | flops | bytes accessed | tf_op | source)
XLA Modules:
  0.0 278.3 jit_solution(9110160832142591906)
XLA Ops:
  9.3 2.8 scatter_fusion
  12.7 7.4 %all-to-all-start = ((s32[16,1,6]{2,1,0:T(1,128)}), s32[16,1,6]{2,1,0:T(1,128)S(1)}, u32[]{:S(2)}, u32[]{:S(2)}) async-start(s32[16,1,6]{2,1,0:T(1,128)} %copy.32), calls=%async_computation | async-start | bytes 16384 | tf_op jit(solution)/shard_map/all_to_all | solution.py:102
  20.1 12.3 %all_gather.3 = bf16[384,1024]{1,0:T(8,128)(2,1)S(1)} all-gather(bf16[384,512]{1,0:T(8,128)(2,1)} %param.8), channel_id=1, replica_groups=mesh['kv'=16,'tp'=2] {'tp'}, dimensions={1}, use_global_device_ids=true | all-gather | bytes 1179648 | tf_op jit(solution)/shard_map/all_gather | solution.py:16
  34.4 8.4 %gather_fusion.2 = bf16[96,64,4,64]{3,2,1,0:T(4,128)(2,1)} fusion(bf16[6,64,4,64]{3,2,1,0:T(4,128)(2,1)S(1)} %reshape.166, s32[1024]{0:T(1024)S(1)} %pad_clamp_fusion), kind=kCustom, calls=%fused_computation.2 | custom fusion | bytes 6291840 | tf_op jit(solution)/shard_map/gather | solution.py:103
  42.8 7.4 %copy.38 = bf16[96,64,4,64]{3,1,2,0:T(8,128)(2,1)} copy(bf16[96,64,4,64]{3,2,1,0:T(4,128)(2,1)} %gather_fusion.2) | data formatting | bytes 6291456 | tf_op jit(solution)/shard_map/gather | solution.py:103
  50.2 12.7 %reshape.208 = bf16[16,2,49152]{2,1,0:T(2,128)(2,1)} reshape(bf16[16,6,4,64,64]{4,3,2,1,0:T(8,128)(2,1)} %bitcast.54) | data formatting | bytes 6291456
  62.9 5.7 %all-to-all-start.2 = ((bf16[16,2,49152]{2,1,0:T(2,128)(2,1)}), bf16[16,2,49152]{2,1,0:T(2,128)(2,1)}, u32[]{:S(2)}, u32[]{:S(2)}) async-start(bf16[16,2,49152]{2,1,0:T(2,128)(2,1)} %reshape.208), calls=%async_computation.2 | async-start | bytes 6291456 | tf_op jit(solution)/shard_map/all_to_all | solution.py:106
  69.2 8.4 %gather_fusion = bf16[96,64,4,64]{3,2,1,0:T(4,128)(2,1)} fusion(bf16[6,64,4,64]{3,2,1,0:T(4,128)(2,1)S(1)} %reshape.161, s32[1024]{0:T(1024)S(1)} %pad_clamp_fusion), kind=kCustom, calls=%fused_computation | custom fusion | bytes 6291840 | tf_op jit(solution)/shard_map/gather | solution.py:104
  77.6 7.4 %copy.35 = bf16[96,64,4,64]{3,1,2,0:T(8,128)(2,1)} copy(bf16[96,64,4,64]{3,2,1,0:T(4,128)(2,1)} %gather_fusion) | data formatting | bytes 6291456 | tf_op jit(solution)/shard_map/gather | solution.py:104
  85.0 12.7 %reshape.210 = bf16[16,2,49152]{2,1,0:T(2,128)(2,1)} reshape(bf16[16,6,4,64,64]{4,3,2,1,0:T(8,128)(2,1)} %bitcast.55) | data formatting | bytes 6291456
  97.7 30.7 %all-to-all-done.2 = bf16[16,2,49152]{2,1,0:T(2,128)(2,1)} async-done(((bf16[16,2,49152]{2,1,0:T(2,128)(2,1)}), bf16[16,2,49152]{2,1,0:T(2,128)(2,1)}, u32[]{:S(2)}, u32[]{:S(2)}) %all-to-all-start.2) | async-done | bytes 3145760 | tf_op jit(solution)/shard_map/all_to_all | solution.py:106
  128.4 15.5 %all-to-all-start.1 = ((bf16[16,2,49152]{2,1,0:T(2,128)(2,1)}), bf16[16,2,49152]{2,1,0:T(2,128)(2,1)}, u32[]{:S(2)}, u32[]{:S(2)}) async-start(bf16[16,2,49152]{2,1,0:T(2,128)(2,1)} %reshape.210), calls=%async_computation.1 | async-start | bytes 6291456 | tf_op jit(solution)/shard_map/all_to_all | solution.py:109
  146.3 12.3 %reshape.209 = bf16[16,6,4,64,64]{4,3,2,1,0:T(8,128)(2,1)} reshape(bf16[16,2,49152]{2,1,0:T(2,128)(2,1)} %all-to-all-done.2) | data formatting | bytes 6291456
  158.6 5.6 %gather_fusion.3 = bf16[48,64,4,64]{3,1,2,0:T(8,128)(2,1)} fusion(bf16[16,6,64,4,64]{4,2,3,1,0:T(8,128)(2,1)} %bitcast.57, s32[48]{0:T(128)S(1)} %bitcast.61), kind=kCustom, calls=%fused_computation.3 | custom fusion | bytes 3146112 | tf_op jit(solution)/shard_map/gather | solution.py:113
  164.3 2.9 %pad_maximum_fusion = bf16[6,9,64,4,64]{4,2,1,3,0:T(8,128)(2,1)S(1)} fusion(bf16[6,1,64,4,64]{4,2,1,3,0:T(8,128)(2,1)S(1)} %copy.39, bf16[6,8,64,4,64]{4,2,3,1,0:T(8,128)(2,1)} %bitcast.59), kind=kLoop, calls=%fused_computation.13 | loop fusion | flops 3538944 | bytes 3538944 | tf_op jit(solution)/shard_map/concatenate | solution.py:119
  169.4 1.8 copy-done.1
  171.2 2.0 fusion.1
  173.2 30.4 %all-to-all-done.1 = bf16[16,2,49152]{2,1,0:T(2,128)(2,1)} async-done(((bf16[16,2,49152]{2,1,0:T(2,128)(2,1)}), bf16[16,2,49152]{2,1,0:T(2,128)(2,1)}, u32[]{:S(2)}, u32[]{:S(2)}) %all-to-all-start.1) | async-done | bytes 3145760 | tf_op jit(solution)/shard_map/all_to_all | solution.py:109
  203.7 12.3 %reshape.211 = bf16[16,6,4,64,64]{4,3,2,1,0:T(8,128)(2,1)} reshape(bf16[16,2,49152]{2,1,0:T(2,128)(2,1)} %all-to-all-done.1) | data formatting | bytes 6291456
  216.0 5.5 %gather_fusion.1 = bf16[48,64,4,64]{3,1,2,0:T(8,128)(2,1)} fusion(bf16[16,6,64,4,64]{4,2,3,1,0:T(8,128)(2,1)} %bitcast.58, s32[48]{0:T(128)S(1)} %bitcast.62), kind=kCustom, calls=%fused_computation.1 | custom fusion | bytes 3146112 | tf_op jit(solution)/shard_map/gather | solution.py:116
  221.6 4.7 %copy.37 = bf16[6,8,64,4,64]{2,4,1,3,0:T(8,128)(2,1)} copy(bf16[6,8,64,4,64]{4,2,3,1,0:T(8,128)(2,1)} %bitcast.60) | data formatting | bytes 3145728 | tf_op jit(solution)/shard_map/reshape | solution.py:116
  226.2 10.3 %multiply_reduce_fusion = (f32[6,64]{1,0:T(8,128)S(1)}, f32[6,64,4,64]{1,3,2,0:T(8,128)S(1)}) fusion(f32[6,64,4]{1,2,0:T(4,128)S(1)} %bitcast.63, f32[6,4,64,9,64]{2,4,3,1,0:T(8,128)} %bitcast.52, f32[6,4,64]{2,1,0:T(4,128)S(1)} %fusion, pred[6,64,9,64]{1,3,2,0:T(8,128)(4,1)S(1)} %broadcast_compare_fusion, bf16[6,8,64,4,64]{2,4,1,3,0:T(8,128)(2,1)} %copy.37, ...), kind=kOutput, calls=%fused_computation.29 | convolution fusion | flops 684392064 | bytes 5936640 | tf_op jit(solution)/shard_map/bhqct,bcthd->bqhd/dot_general | solution.py:41
  237.4 5.0 %psum.7 = f32[384]{0:T(512)S(1)} all-reduce(f32[384]{0:T(512)S(1)} %reduce_sum.35), channel_id=1, replica_groups=mesh['kv'=16,'tp'=2] {'tp'}, use_global_device_ids=true, to_apply=%region_6.7 | all-reduce | flops 384 | bytes 3072 | tf_op jit(solution)/shard_map/psum | solution.py:130
  243.7 27.8 %reduce-scatter.2.cloned.1.call-done = bf16[512,384]{0,1:T(8,128)(2,1)} async-done(((bf16[1024,384]{0,1:T(8,128)(2,1)}), bf16[512,384]{0,1:T(8,128)(2,1)}) %reduce-scatter.2.cloned.1.call-update) | async-done | bytes 393232 | tf_op jit(solution)/shard_map/reduce_scatter | solution.py:27
  (48 shorter events, 12.5 us)
Async XLA Ops:
  6.5 235.8 %copy-start = (bf16[256,1024]{1,0:T(8,128)(2,1)S(1)}, bf16[256,1024]{1,0:T(8,128)(2,1)}, u32[]{:S(2)}) copy-start(bf16[256,1024]{1,0:T(8,128)(2,1)} %param.12) | copy-start | bytes 1572868
  12.7 21.4 %all-to-all-start = ((s32[16,1,6]{2,1,0:T(1,128)}), s32[16,1,6]{2,1,0:T(1,128)S(1)}, u32[]{:S(2)}, u32[]{:S(2)}) async-start(s32[16,1,6]{2,1,0:T(1,128)} %copy.32), calls=%async_computation | async-start | bytes 16384 | tf_op jit(solution)/shard_map/all_to_all | solution.py:102
  50.2 18.4 %copy-start.2 = (bf16[1024,256]{1,0:T(8,128)(2,1)S(1)}, bf16[1024,256]{1,0:T(8,128)(2,1)}, u32[]{:S(2)}) copy-start(bf16[1024,256]{1,0:T(8,128)(2,1)} %param.11) | copy-start | bytes 1572868
  62.9 65.5 %all-to-all-start.2 = ((bf16[16,2,49152]{2,1,0:T(2,128)(2,1)}), bf16[16,2,49152]{2,1,0:T(2,128)(2,1)}, u32[]{:S(2)}, u32[]{:S(2)}) async-start(bf16[16,2,49152]{2,1,0:T(2,128)(2,1)} %reshape.208), calls=%async_computation.2 | async-start | bytes 6291456 | tf_op jit(solution)/shard_map/all_to_all | solution.py:106
  97.7 46.9 %copy-start.3 = (bf16[1024,256]{1,0:T(8,128)(2,1)S(1)}, bf16[1024,256]{1,0:T(8,128)(2,1)}, u32[]{:S(2)}) copy-start(bf16[1024,256]{1,0:T(8,128)(2,1)} %param.9) | copy-start | bytes 1572868
  128.4 75.3 %all-to-all-start.1 = ((bf16[16,2,49152]{2,1,0:T(2,128)(2,1)}), bf16[16,2,49152]{2,1,0:T(2,128)(2,1)}, u32[]{:S(2)}, u32[]{:S(2)}) async-start(bf16[16,2,49152]{2,1,0:T(2,128)(2,1)} %reshape.210), calls=%async_computation.1 | async-start | bytes 6291456 | tf_op jit(solution)/shard_map/all_to_all | solution.py:109
  143.9 127.6 %reduce-scatter.2.cloned.1.call-start = ((), (), s32[]{:S(2)}) async-start(), calls=%async_computation.4 | async-start | bytes 1179648 | tf_op jit(solution)/shard_map/reduce_scatter | solution.py:27
  168.3 2.9 %copy-start.1 = (f32[6,4,64,576]{2,3,1,0}, f32[6,4,64,576]{2,3,1,0:S(1)}, u32[]{:S(2)}) copy-start(f32[6,4,64,576]{2,3,1,0:S(1)} %fusion.24) | copy-start | bytes 10616836
  226.2 16.1 %copy-start.4 = (f32[256]{0:T(256)S(1)}, f32[256]{0:T(256)}, u32[]{:S(2)}) copy-start(f32[256]{0:T(256)} %param.13) | copy-start | bytes 3076
Sparse Core Ops, SparseCore 0:
  243.8 27.6 reduce-scatter.1
where the time goes:
time: 280 us; the launch traced here: 278 us
  local copies, waits for them, and re-layouts  108 us (39%)
  waiting for transfers between devices  88.9 us (32%)
  starting transfers between devices  28.9 us (10%)
  blocking collectives  17.2 us (6%)
  matrix products  14.8 us (5%)
  between operations  13.6 us (5%)
  other arithmetic  7.16 us (3%)
    unnamed x14, local copies, waits for them, and re-layouts  51.9 us
    all_to_all x1, waiting for transfers between devices, on_device(): lax.all_to_all(for_sending(key_pack), 'kv', split_axis=0, concat_axis=0,...  30.7 us
    all_to_all x1, waiting for transfers between devices, on_device(): lax.all_to_all(for_sending(value_pack), 'kv', split_axis=0, concat_axis=0...  30.4 us
    reduce_scatter x1, waiting for transfers between devices, scattered(): lax.psum_scatter(sent, axis, scatter_dimension=0, tiled=True)  27.8 us
    gather x2, local copies, waits for them, and re-layouts, on_device(): value_pack = local_values[incoming]  15.8 us
    gather x2, local copies, waits for them, and re-layouts, on_device(): key_pack = local_keys[incoming]  15.8 us
    all_to_all x1, starting transfers between devices, on_device(): lax.all_to_all(for_sending(value_pack), 'kv', split_axis=0, concat_axis=0...  15.5 us
    all_gather x1, blocking collectives, folded(): lax.all_gather(part, axis, axis=dim, tiled=True)  12.3 us
  transfers between devices with their start and end apart: 4, of which 3 were waited for; matrix products, arithmetic and copies ran while one was open for 21% of the time, Pallas kernels for 0%

commit v1 on v0

--- a/solution.py
+++ b/solution.py
@@ -1,6 +1,10 @@
+import functools
+
 import jax
 import jax.numpy as jnp
 from jax import lax
+from jax.experimental import pallas as pl
+from jax.experimental.pallas import tpu as pltpu
 from jax.sharding import PartitionSpec as P
 
 HEADS = 8
@@ -140,9 +144,347 @@
     return summed.T.astype(jnp.bfloat16)
 
 
+MESH_ID = pl.DeviceIdType.MESH
+CORES = 2
+
+
+def kv_grid(kv_count):
+    chips = kv_count // CORES
+    along_y = 1 << ((chips.bit_length() - 1) // 2)
+    return chips // along_y, along_y
+
+
+def swap_half(value):
+    return pltpu.roll(value, value.shape[-1] // 2, 1)
+
+
+def interleave(first, second):
+    low = lax.broadcasted_iota(jnp.int32, first.shape, 1) < first.shape[-1] // 2
+    return jnp.where(low, first, swap_half(second)), jnp.where(low, swap_half(first), second)
+
+
+def fused_kernel(
+    nz, ny, tok, wq, wk, wv, wo, gain, owner, local, out,
+    tokp, acc, kv, kvs, qs, qbuf, att, ats, wp, gp, cst, cb, cs,
+    tok_s, tok_r, w_s, w_r, g_s, g_r, c_s, c_r, zk_s, zk_r, zq_s, zq_r,
+    yk_s, yk_r, dk_s, dk_r, rt_s, rt_r, xa_s, xa_r, loc_sem,
+):
+    me = lax.axis_index("kv")
+    x = lax.axis_index("tp")
+    z = me // (ny * CORES)
+    y = (me // CORES) % ny
+    c = me % CORES
+    rows, feats = tok.shape
+    blocks = rows // BLOCK
+    pairs = blocks // 2
+    heads = wq.shape[1] // HEAD_SIZE
+    hw = heads * HEAD_SIZE
+    wide = 2 * HEAD_SIZE
+    cols = out.shape[1]
+
+    def dev(zz, yy, cc):
+        return (zz * ny + yy) * CORES + cc
+
+    def zfrom(d):
+        return (z + nz - d) % nz
+
+    def zto(d):
+        return (z + d) % nz
+
+    def push(src, dst, ss, rs, kv_id, tp_id):
+        return pltpu.make_async_remote_copy(
+            src_ref=src, dst_ref=dst, send_sem=ss, recv_sem=rs,
+            device_id={"kv": kv_id, "tp": tp_id}, device_id_type=MESH_ID,
+        )
+
+    barrier = pltpu.get_barrier_semaphore()
+    peers = [(me, 1 - x), (dev(z, 1 - y, c), x), (dev(z, y, 1 - c), x)]
+    peers += [(dev(zto(d), y, c), x) for d in range(1, nz)]
+    for kv_id, tp_id in peers:
+        pl.semaphore_signal(
+            barrier, inc=1, device_id={"kv": kv_id, "tp": tp_id}, device_id_type=MESH_ID
+        )
+    cst[...] = jnp.zeros(cst.shape, jnp.int32)
+    cst[0:blocks, 0 : owner.shape[1]] = owner[...] * blocks + local[...]
+    pl.semaphore_wait(barrier, len(peers))
+
+    def tok_copy(k):
+        part = pl.ds(k * 2 * BLOCK, 2 * BLOCK)
+        return push(tok.at[part], tokp.at[part], tok_s.at[k], tok_r.at[k], me, 1 - x)
+
+    def w_copy():
+        theirs = pl.ds(pl.multiple_of((1 - x) * cols, 128), cols)
+        return push(wo.at[:, theirs], wp, w_s, w_r, me, 1 - x)
+
+    def g_copy():
+        return push(gain, gp, g_s, g_r, me, 1 - x)
+
+    def c_copy(d):
+        return push(cst, cb.at[d], c_s.at[d], c_r.at[d], dev(zto(d), y, c), x)
+
+    def zk_copy(d, k):
+        part = pl.ds(2 * k, 2)
+        return push(
+            kvs.at[zto(d), part], kv.at[pl.ds(me * blocks + 2 * k, 2)],
+            zk_s.at[d, k], zk_r.at[d, k], dev(zto(d), y, c), x,
+        )
+
+    def zq_copy(d, k):
+        return push(
+            qs.at[zto(d), k], qbuf.at[d, k], zq_s.at[d, k], zq_r.at[d, k], dev(zto(d), y, c), x
+        )
+
+    def slot(d, yy, k):
+        return kv.at[pl.ds(dev(zfrom(d), yy, c) * blocks + 2 * k, 2)]
+
+    def yk_copy(d, k):
+        part = slot(d, y, k)
+        return push(part, part, yk_s.at[d, k], yk_r.at[d, k], dev(z, 1 - y, c), x)
+
+    def dk_copy(side, d, k):
+        part = slot(d, y if side == 0 else 1 - y, k)
+        return push(
+            part, part, dk_s.at[side, d, k], dk_r.at[side, d, k], dev(z, y, 1 - c), x
+        )
+
+    def rt_copy(d, p):
+        return push(
+            ats.at[d, p], att.at[x, z, p], rt_s.at[d, p], rt_r.at[d, p], dev(zfrom(d), y, c), x
+        )
+
+    def xa_copy(d, p):
+        part = att.at[x, zto(d), p]
+        return push(part, part, xa_s.at[d, p], xa_r.at[d, p], me, 1 - x)
+
+    for k in range(pairs):
+        tok_copy(k).start()
+    w_copy().start()
+    g_copy().start()
+    for d in range(1, nz):
+        c_copy(d).start()
+    cb[0] = cst[...]
+
+    mine = pl.ds(pl.multiple_of(x * feats, 128), feats)
+    theirs = pl.ds(pl.multiple_of((1 - x) * feats, 128), feats)
+    for at, weight in enumerate((wq, wk, wv)):
+        acc[:, at * hw : (at + 1) * hw] = jnp.dot(
+            tok[...], weight[mine, :], preferred_element_type=jnp.float32
+        )
+
+    scale = HEAD_SIZE**-0.5
+    for k in range(pairs):
+        tok_copy(k).wait_recv()
+        span = slice(2 * k * BLOCK, (2 * k + 2) * BLOCK)
+        got = []
+        for at, weight in enumerate((wq, wk, wv)):
+            got.append(
+                acc[span, at * hw : (at + 1) * hw]
+                + jnp.dot(
+                    tokp[span, :], weight[theirs, :], preferred_element_type=jnp.float32
+                )
+            )
+        q, key, val = got
+        for j in range(heads // 2):
+            lanes = slice(j * wide, (j + 1) * wide)
+            even, odd = interleave(key[:, lanes], val[:, lanes])
+            for h, both in ((2 * j, even), (2 * j + 1, odd)):
+                kvs[h, 2 * k : 2 * k + 2] = both.astype(jnp.bfloat16).reshape(2, BLOCK, wide)
+        kv[pl.ds(me * blocks + 2 * k, 2)] = kvs[z, 2 * k : 2 * k + 2]
+        for d in sorted(range(1, nz), key=lambda d: abs(2 * d - nz)):
+            zk_copy(d, k).start()
+        yk_copy(0, k).start()
+        dk_copy(0, 0, k).start()
+        for j in range(heads // 2):
+            lanes = slice(j * wide, (j + 1) * wide)
+            even, odd = interleave(q[:BLOCK, lanes], q[BLOCK:, lanes])
+            qs[2 * j, k] = (even.astype(jnp.bfloat16) * scale).astype(jnp.bfloat16)
+            qs[2 * j + 1, k] = (odd.astype(jnp.bfloat16) * scale).astype(jnp.bfloat16)
+        qbuf[0, k] = qs[z, k]
+        for d in range(1, nz):
+            zq_copy(d, k).start()
+
+    order = [(d, k) for k in range(pairs) for d in range(nz)]
+    lag = nz
+    for at in range(len(order) + lag):
+        if at < len(order):
+            d, k = order[at]
+            if d > 0:
+                zk_copy(d, k).wait_recv()
+                yk_copy(d, k).start()
+                dk_copy(0, d, k).start()
+        if at >= lag:
+            d, k = order[at - lag]
+            yk_copy(d, k).wait_recv()
+            dk_copy(1, d, k).start()
+    for d in range(1, nz):
+        c_copy(d).wait_recv()
+        for k in range(pairs):
+            zq_copy(d, k).wait_recv()
+    to_scalar = pltpu.make_async_copy(cb, cs, loc_sem)
+    to_scalar.start()
+    to_scalar.wait()
+    for d, k in order:
+        for side in range(2):
+            dk_copy(side, d, k).wait_recv()
+
+    chosen = owner.shape[1]
+    listed = (chosen + 1) * BLOCK
+    row_at = lax.broadcasted_iota(jnp.int32, (BLOCK, listed), 0)
+    col_at = lax.broadcasted_iota(jnp.int32, (BLOCK, listed), 1)
+    visible = (col_at <= row_at) | (col_at >= BLOCK)
+    low = lax.broadcasted_iota(jnp.int32, (BLOCK, wide), 1) < HEAD_SIZE
+
+    def attend(query, d, b):
+        own = dev(zfrom(d), y, c) * blocks + b
+        pieces = [kv[own]] + [kv[cs[d, b, j]] for j in range(chosen)]
+        both = jnp.concatenate(pieces, axis=0)
+        scores = lax.dot_general(
+            query, both, (((1,), (1,)), ((), ())), preferred_element_type=jnp.float32
+        )
+        scores = jnp.where(visible, scores, neg_fill)
+        highest = jnp.max(scores, axis=1, keepdims=True)
+        weights = jnp.exp(scores - highest)
+        mass = jnp.sum(weights, axis=1, keepdims=True)
+        blended = jnp.dot(weights.astype(jnp.bfloat16), both, preferred_element_type=jnp.float32)
+        return blended / mass
+
+    def pair_of(d, p):
+        packed = qbuf[d, p].astype(jnp.float32)
+        nothing = jnp.zeros_like(packed)
+        first = jnp.where(low, packed, nothing).astype(jnp.bfloat16)
+        second = jnp.where(low, swap_half(packed), nothing).astype(jnp.bfloat16)
+        first = attend(first, d, 2 * p)
+        second = attend(second, d, 2 * p + 1)
+        return jnp.where(low, swap_half(first), second).astype(jnp.bfloat16)
+
+    def pass_on(d):
+        for p in range(pairs):
+            rt_copy(d, p).wait_recv()
+            xa_copy(d, p).start()
+
+    sequence = list(range(nz - 1, -1, -1))
+    for turn, d in enumerate(sequence):
+
+        def one(p, carry, d=d):
+            if d == 0:
+                att[x, z, p] = pair_of(d, p)
+                xa_copy(d, p).start()
+            else:
+                ats[d, p] = pair_of(d, p)
+                rt_copy(d, p).start()
+            return carry
+
+        lax.fori_loop(0, pairs, one, 0)
+        if turn >= 2:
+            pass_on(sequence[turn - 2])
+    for d in sequence[-2:]:
+        if d > 0:
+            pass_on(d)
+
+    w_copy().wait_recv()
+    g_copy().wait_recv()
+    mine_cols = pl.ds(pl.multiple_of(x * cols, 128), cols)
+    for p in range(pairs):
+        for d in range(nz):
+            xa_copy(d, p).wait_recv()
+        halves = []
+        for side in (x, 1 - x):
+            upper, lower = [], []
+            for j in range(heads // 2):
+                up, down = interleave(
+                    att[side, 2 * j, p].astype(jnp.float32),
+                    att[side, 2 * j + 1, p].astype(jnp.float32),
+                )
+                upper.append(up)
+                lower.append(down)
+            halves.append(
+                jnp.concatenate(
+                    [jnp.concatenate(upper, axis=1), jnp.concatenate(lower, axis=1)], axis=0
+                )
+            )
+        squares = sum(jnp.sum(half * half, axis=1, keepdims=True) for half in halves)
+        inverse = lax.rsqrt(squares / (2 * hw) + eps_norm)
+        normed = [
+            (half * inverse * g[...]).astype(jnp.bfloat16) for half, g in zip(halves, (gain, gp))
+        ]
+        total = jnp.dot(normed[0], wo[:, mine_cols], preferred_element_type=jnp.float32)
+        total += jnp.dot(normed[1], wp[...], preferred_element_type=jnp.float32)
+        out[2 * p * BLOCK : (2 * p + 2) * BLOCK, :] = total.astype(jnp.bfloat16)
+
+    for k in range(pairs):
+        tok_copy(k).wait_send()
+    w_copy().wait_send()
+    g_copy().wait_send()
+    for d in range(nz):
+        if d > 0:
+            c_copy(d).wait_send()
+        for k in range(pairs):
+            if d > 0:
+                zk_copy(d, k).wait_send()
+                zq_copy(d, k).wait_send()
+                rt_copy(d, k).wait_send()
+            yk_copy(d, k).wait_send()
+            dk_copy(0, d, k).wait_send()
+            dk_copy(1, d, k).wait_send()
+            xa_copy(d, k).wait_send()
+
+
+def fused(nz, ny, tok, wq, wk, wv, wo, gain, owner, local):
+    rows, feats = tok.shape
+    blocks = rows // BLOCK
+    pairs = blocks // 2
+    heads = wq.shape[1] // HEAD_SIZE
+    hw = heads * HEAD_SIZE
+    cols = wo.shape[1] // 2
+    wide = 2 * HEAD_SIZE
+    everyone = nz * ny * CORES * blocks
+    bf16 = jnp.bfloat16
+    vmem, dma = pltpu.VMEM, pltpu.SemaphoreType.DMA
+    two = lambda shape: [dma(shape), dma(shape)]
+    scratch = [
+        vmem((rows, feats), bf16),
+        vmem((rows, 3 * hw), jnp.float32),
+        vmem((everyone, BLOCK, wide), bf16),
+        vmem((heads, blocks, BLOCK, wide), bf16),
+        vmem((heads, pairs, BLOCK, wide), bf16),
+        vmem((nz, pairs, BLOCK, wide), bf16),
+        vmem((2, heads, pairs, BLOCK, wide), bf16),
+        vmem((nz, pairs, BLOCK, wide), bf16),
+        vmem((hw, cols), bf16),
+        vmem((1, hw), jnp.float32),
+        vmem((8, 128), jnp.int32),
+        vmem((nz, 8, 128), jnp.int32),
+        pltpu.SMEM((nz, 8, 128), jnp.int32),
+    ]
+    scratch += two((pairs,)) + two(()) + two(()) + two((nz,))
+    scratch += two((nz, pairs)) * 3 + two((2, nz, pairs)) + two((nz, pairs)) * 2 + [dma(())]
+    return pl.pallas_call(
+        functools.partial(fused_kernel, nz, ny),
+        out_shape=jax.ShapeDtypeStruct((rows, cols), bf16),
+        in_specs=[pl.BlockSpec(memory_space=pltpu.VMEM)] * 8,
+        out_specs=pl.BlockSpec(memory_space=pltpu.VMEM),
+        scratch_shapes=scratch,
+        compiler_params=pltpu.CompilerParams(collective_id=0, has_side_effects=True),
+    )(tok, wq, wk, wv, wo, gain.reshape(1, hw), owner, local)
+
+
 def solution(mesh):
+    kv_count, tp_count = mesh.shape["kv"], mesh.shape["tp"]
+    nz, ny = kv_grid(kv_count)
+
+    def step(tokens, *rest):
+        blocks = tokens.shape[0] // BLOCK
+        heads = rest[0].shape[1] // HEAD_SIZE
+        fits = (
+            tp_count == 2 and ny == 2 and nz == heads and blocks % 2 == 0 and blocks <= 8
+            and nz * ny * CORES == kv_count and 2 * HEAD_SIZE == 128
+        )
+        if fits:
+            return fused(nz, ny, tokens, *rest)
+        return on_device(tokens, *rest)
+
     return jax.shard_map(
-        on_device,
+        step,
         mesh=mesh,
         in_specs=(
             P("kv", "tp"),

time: 280 us -> 47.6 us (0.17)
  local copies, waits for them, and re-layouts: 108 us -> 1.77 us
  waiting for transfers between devices: 88.9 us -> 0 us
  Pallas kernels: 0 us -> 45.7 us
  starting transfers between devices: 28.9 us -> 0 us
  blocking collectives: 17.2 us -> 0 us
  matrix products: 14.8 us -> 0 us
  between operations: 13.6 us -> 0.01 us
  other arithmetic: 7.16 us -> 0 us
    all_to_all x3 -> x0, waiting for transfers between devices: 61.1 us -> none  [the longest x1 30.7 us: on_device(): lax.all_to_all(for_sending(key_pack), 'kv', split_axis=0, concat_axis=0,...]
    unnamed x14 -> x1, local copies, waits for them, and re-layouts: 51.9 us -> 1.77 us
    pallas_call x0 -> x1, Pallas kernels: none -> 45.7 us  [fused(): pl.pallas_call(functools.partial(fused_kernel, nz, ny), out_shape=jax.Sha...]
    gather x6 -> x0, local copies, waits for them, and re-layouts: 42.8 us -> none  [the longest x2 15.8 us: on_device(): value_pack = local_values[incoming]]
    all_to_all x3 -> x0, starting transfers between devices: 28.6 us -> none  [the longest x1 15.5 us: on_device(): lax.all_to_all(for_sending(value_pack), 'kv', split_axis=0, concat_axis=0...]
    reduce_scatter x1 -> x0, waiting for transfers between devices: 27.8 us -> none  [scattered(): lax.psum_scatter(sent, axis, scatter_dimension=0, tiled=True)]
    dot_general x5 -> x0, matrix products: 13.8 us -> none  [the longest x1 10.3 us: partial_softmax(): jnp.einsum('bhqct,bcthd->bqhd', weights, value_rows.astype(jnp.float32),...]
    all_gather x1 -> x0, blocking collectives: 12.3 us -> none  [folded(): lax.all_gather(part, axis, axis=dim, tiled=True)]
  transfers between devices with their start and end apart: 4 -> 0, of which waited for: 3 -> 0; matrix products, arithmetic and copies ran while one was open for 21% -> 0% of each run, Pallas kernels for 0% -> 0%
where the time goes in v1:
time: 47.6 us; the launch traced here: 47.4 us
  Pallas kernels  45.7 us (96%)
  local copies, waits for them, and re-layouts  1.77 us (4%)
    pallas_call x1, Pallas kernels, fused(): pl.pallas_call(functools.partial(fused_kernel, nz, ny), out_shape=jax.Sha...  45.7 us
    unnamed x1, local copies, waits for them, and re-layouts  1.77 us

profile of v1, /device:TPU:0, one launch (start us, length us, event | category | flops | bytes accessed | tf_op | source)
XLA Modules:
  0.0 47.4 jit_solution(877964024433624889)
XLA Ops:
  0.0 45.7 %shard_map.82 = bf16[384,512]{1,0:T(8,128)(2,1)} custom-call(bf16[384,512]{1,0:T(8,128)(2,1)} %tok.1, bf16[1024,256]{1,0:T(8,128)(2,1)} %wq.1, bf16[1024,256]{1,0:T(8,128)(2,1)} %wk.1, bf16[1024,256]{1,0:T(8,128)(2,1)} %wv.1, bf16[256,1024]{1,0:T(8,128)(2,1)} %wo.1, f32[1,256]{1,0:T(1,128)} %bitcast.1, s32[6,8]{1,0:T(8,128)} %owner.1, s32[6,8]{1,0:T(8,128)} %local.1), custom_call_target="tpu_custom_call" | custom-call | tf_op jit(solution)/shard_map/pallas_call | solution.py:461
  45.7 1.8 %copy.10 = bf16[384,512]{1,0:T(8,128)(2,1)} copy(bf16[384,512]{1,0:T(8,128)(2,1)} %shard_map.82) | data formatting | bytes 786432

commit v2 on v1

--- a/solution.py
+++ b/solution.py
@@ -154,6 +154,10 @@
     return chips // along_y, along_y
 
 
+def chunk_spans(blocks):
+    return [(0, 1), (1, 1)] + [(b, 2) for b in range(2, blocks, 2)]
+
+
 def swap_half(value):
     return pltpu.roll(value, value.shape[-1] // 2, 1)
 
@@ -177,6 +181,8 @@
     rows, feats = tok.shape
     blocks = rows // BLOCK
     pairs = blocks // 2
+    spans = chunk_spans(blocks)
+    chunks = range(len(spans))
     heads = wq.shape[1] // HEAD_SIZE
     hw = heads * HEAD_SIZE
     wide = 2 * HEAD_SIZE
@@ -206,10 +212,16 @@
         )
     cst[...] = jnp.zeros(cst.shape, jnp.int32)
     cst[0:blocks, 0 : owner.shape[1]] = owner[...] * blocks + local[...]
+    mine = pl.ds(pl.multiple_of(x * feats, 128), feats)
+    theirs = pl.ds(pl.multiple_of((1 - x) * feats, 128), feats)
+    for at, weight in enumerate((wq, wk, wv)):
+        acc[:, at * hw : (at + 1) * hw] = jnp.dot(
+            tok[...], weight[mine, :], preferred_element_type=jnp.float32
+        )
     pl.semaphore_wait(barrier, len(peers))
 
     def tok_copy(k):
-        part = pl.ds(k * 2 * BLOCK, 2 * BLOCK)
+        part = pl.ds(spans[k][0] * BLOCK, spans[k][1] * BLOCK)
         return push(tok.at[part], tokp.at[part], tok_s.at[k], tok_r.at[k], me, 1 - x)
 
     def w_copy():
@@ -223,19 +235,17 @@
         return push(cst, cb.at[d], c_s.at[d], c_r.at[d], dev(zto(d), y, c), x)
 
     def zk_copy(d, k):
-        part = pl.ds(2 * k, 2)
+        at, many = spans[k]
         return push(
-            kvs.at[zto(d), part], kv.at[pl.ds(me * blocks + 2 * k, 2)],
+            kvs.at[zto(d), pl.ds(at, many)], kv.at[pl.ds(me * blocks + at, many)],
             zk_s.at[d, k], zk_r.at[d, k], dev(zto(d), y, c), x,
         )
 
-    def zq_copy(d, k):
-        return push(
-            qs.at[zto(d), k], qbuf.at[d, k], zq_s.at[d, k], zq_r.at[d, k], dev(zto(d), y, c), x
-        )
+    def zq_copy(d):
+        return push(qs.at[zto(d)], qbuf.at[d], zq_s.at[d], zq_r.at[d], dev(zto(d), y, c), x)
 
     def slot(d, yy, k):
-        return kv.at[pl.ds(dev(zfrom(d), yy, c) * blocks + 2 * k, 2)]
+        return kv.at[pl.ds(dev(zfrom(d), yy, c) * blocks + spans[k][0], spans[k][1])]
 
     def yk_copy(d, k):
         part = slot(d, y, k)
@@ -256,7 +266,7 @@
         part = att.at[x, zto(d), p]
         return push(part, part, xa_s.at[d, p], xa_r.at[d, p], me, 1 - x)
 
-    for k in range(pairs):
+    for k in chunks:
         tok_copy(k).start()
     w_copy().start()
     g_copy().start()
@@ -264,68 +274,80 @@
         c_copy(d).start()
     cb[0] = cst[...]
 
-    mine = pl.ds(pl.multiple_of(x * feats, 128), feats)
-    theirs = pl.ds(pl.multiple_of((1 - x) * feats, 128), feats)
-    for at, weight in enumerate((wq, wk, wv)):
-        acc[:, at * hw : (at + 1) * hw] = jnp.dot(
-            tok[...], weight[mine, :], preferred_element_type=jnp.float32
-        )
-
     scale = HEAD_SIZE**-0.5
-    for k in range(pairs):
+    far_first = sorted(range(1, nz), key=lambda d: abs(2 * d - nz))
+
+    def rest(at, weight, span):
+        return acc[span, at * hw : (at + 1) * hw] + jnp.dot(
+            tokp[span, :], weight[theirs, :], preferred_element_type=jnp.float32
+        )
+
+    def keys_out(k):
+        at, many = spans[k]
         tok_copy(k).wait_recv()
-        span = slice(2 * k * BLOCK, (2 * k + 2) * BLOCK)
-        got = []
-        for at, weight in enumerate((wq, wk, wv)):
-            got.append(
-                acc[span, at * hw : (at + 1) * hw]
-                + jnp.dot(
-                    tokp[span, :], weight[theirs, :], preferred_element_type=jnp.float32
-                )
-            )
-        q, key, val = got
+        span = slice(at * BLOCK, (at + many) * BLOCK)
+        key, val = rest(1, wk, span), rest(2, wv, span)
         for j in range(heads // 2):
             lanes = slice(j * wide, (j + 1) * wide)
             even, odd = interleave(key[:, lanes], val[:, lanes])
             for h, both in ((2 * j, even), (2 * j + 1, odd)):
-                kvs[h, 2 * k : 2 * k + 2] = both.astype(jnp.bfloat16).reshape(2, BLOCK, wide)
-        kv[pl.ds(me * blocks + 2 * k, 2)] = kvs[z, 2 * k : 2 * k + 2]
-        for d in sorted(range(1, nz), key=lambda d: abs(2 * d - nz)):
+                kvs[h, at : at + many] = both.astype(jnp.bfloat16).reshape(many, BLOCK, wide)
+        for d in far_first:
             zk_copy(d, k).start()
+        kv[pl.ds(me * blocks + at, many)] = kvs[z, at : at + many]
         yk_copy(0, k).start()
         dk_copy(0, 0, k).start()
+
+    def queries_out():
+        q = rest(0, wq, slice(0, rows))
         for j in range(heads // 2):
             lanes = slice(j * wide, (j + 1) * wide)
-            even, odd = interleave(q[:BLOCK, lanes], q[BLOCK:, lanes])
-            qs[2 * j, k] = (even.astype(jnp.bfloat16) * scale).astype(jnp.bfloat16)
-            qs[2 * j + 1, k] = (odd.astype(jnp.bfloat16) * scale).astype(jnp.bfloat16)
-        qbuf[0, k] = qs[z, k]
+            for k in range(pairs):
+                first = q[2 * k * BLOCK : (2 * k + 1) * BLOCK, lanes]
+                second = q[(2 * k + 1) * BLOCK : (2 * k + 2) * BLOCK, lanes]
+                even, odd = interleave(first, second)
+                qs[2 * j, k] = (even.astype(jnp.bfloat16) * scale).astype(jnp.bfloat16)
+                qs[2 * j + 1, k] = (odd.astype(jnp.bfloat16) * scale).astype(jnp.bfloat16)
+        for d in far_first:
+            zq_copy(d).start()
+        qbuf[0] = qs[z]
+
+    def relay_z(k):
         for d in range(1, nz):
-            zq_copy(d, k).start()
-
-    order = [(d, k) for k in range(pairs) for d in range(nz)]
-    lag = nz
-    for at in range(len(order) + lag):
-        if at < len(order):
-            d, k = order[at]
-            if d > 0:
-                zk_copy(d, k).wait_recv()
-                yk_copy(d, k).start()
-                dk_copy(0, d, k).start()
-        if at >= lag:
-            d, k = order[at - lag]
+            zk_copy(d, k).wait_recv()
+            yk_copy(d, k).start()
+            dk_copy(0, d, k).start()
+
+    def relay_y(k):
+        for d in range(nz):
             yk_copy(d, k).wait_recv()
             dk_copy(1, d, k).start()
+
+    last = len(spans) - 1
+    for k in chunks:
+        keys_out(k)
+        if k >= 2:
+            relay_z(k - 2)
+    queries_out()
+    for k in range(max(0, last - 1), last + 1):
+        relay_z(k)
+        if k >= 1:
+            relay_y(k - 1)
+        if k == last - 1:
+            for early in range(k - 1):
+                relay_y(early)
+    relay_y(last)
     for d in range(1, nz):
         c_copy(d).wait_recv()
-        for k in range(pairs):
-            zq_copy(d, k).wait_recv()
     to_scalar = pltpu.make_async_copy(cb, cs, loc_sem)
     to_scalar.start()
     to_scalar.wait()
-    for d, k in order:
-        for side in range(2):
-            dk_copy(side, d, k).wait_recv()
+    for d in range(1, nz):
+        zq_copy(d).wait_recv()
+    for k in chunks:
+        for d in range(nz):
+            for side in range(2):
+                dk_copy(side, d, k).wait_recv()
 
     chosen = owner.shape[1]
     listed = (chosen + 1) * BLOCK
@@ -357,34 +379,28 @@
         second = attend(second, d, 2 * p + 1)
         return jnp.where(low, swap_half(first), second).astype(jnp.bfloat16)
 
-    def pass_on(d):
-        for p in range(pairs):
+    sequence = list(range(nz - 1, -1, -1))
+
+    def work(p):
+        for at in range(0, nz, 2):
+            group = sequence[at : at + 2]
+            done = [pair_of(d, p) for d in group]
+            for d, value in zip(group, done):
+                if d == 0:
+                    att[x, z, p] = value
+                    xa_copy(d, p).start()
+                else:
+                    ats[d, p] = value
+                    rt_copy(d, p).start()
+
+    def pass_on(p):
+        for d in sequence[:-1]:
             rt_copy(d, p).wait_recv()
             xa_copy(d, p).start()
 
-    sequence = list(range(nz - 1, -1, -1))
-    for turn, d in enumerate(sequence):
-
-        def one(p, carry, d=d):
-            if d == 0:
-                att[x, z, p] = pair_of(d, p)
-                xa_copy(d, p).start()
-            else:
-                ats[d, p] = pair_of(d, p)
-                rt_copy(d, p).start()
-            return carry
-
-        lax.fori_loop(0, pairs, one, 0)
-        if turn >= 2:
-            pass_on(sequence[turn - 2])
-    for d in sequence[-2:]:
-        if d > 0:
-            pass_on(d)
-
-    w_copy().wait_recv()
-    g_copy().wait_recv()
     mine_cols = pl.ds(pl.multiple_of(x * cols, 128), cols)
-    for p in range(pairs):
+
+    def finish(p):
         for d in range(nz):
             xa_copy(d, p).wait_recv()
         halves = []
@@ -411,22 +427,38 @@
         total += jnp.dot(normed[1], wp[...], preferred_element_type=jnp.float32)
         out[2 * p * BLOCK : (2 * p + 2) * BLOCK, :] = total.astype(jnp.bfloat16)
 
-    for k in range(pairs):
+    for p in range(pairs):
+        work(p)
+        if p >= 1:
+            pass_on(p - 1)
+    w_copy().wait_recv()
+    g_copy().wait_recv()
+    for p in range(pairs - 1):
+        finish(p)
+        if p == pairs - 2:
+            pass_on(pairs - 1)
+    if pairs == 1:
+        pass_on(0)
+    finish(pairs - 1)
+
+    for k in chunks:
         tok_copy(k).wait_send()
     w_copy().wait_send()
     g_copy().wait_send()
     for d in range(nz):
         if d > 0:
             c_copy(d).wait_send()
-        for k in range(pairs):
+            zq_copy(d).wait_send()
+        for k in chunks:
             if d > 0:
                 zk_copy(d, k).wait_send()
-                zq_copy(d, k).wait_send()
-                rt_copy(d, k).wait_send()
             yk_copy(d, k).wait_send()
             dk_copy(0, d, k).wait_send()
             dk_copy(1, d, k).wait_send()
-            xa_copy(d, k).wait_send()
+        for p in range(pairs):
+            if d > 0:
+                rt_copy(d, p).wait_send()
+            xa_copy(d, p).wait_send()
 
 
 def fused(nz, ny, tok, wq, wk, wv, wo, gain, owner, local):
@@ -456,8 +488,10 @@
         vmem((nz, 8, 128), jnp.int32),
         pltpu.SMEM((nz, 8, 128), jnp.int32),
     ]
-    scratch += two((pairs,)) + two(()) + two(()) + two((nz,))
-    scratch += two((nz, pairs)) * 3 + two((2, nz, pairs)) + two((nz, pairs)) * 2 + [dma(())]
+    many = len(chunk_spans(blocks))
+    scratch += two((many,)) + two(()) + two(()) + two((nz,))
+    scratch += two((nz, many)) + two((nz,)) + two((nz, many)) + two((2, nz, many))
+    scratch += two((nz, pairs)) * 2 + [dma(())]
     return pl.pallas_call(
         functools.partial(fused_kernel, nz, ny),
         out_shape=jax.ShapeDtypeStruct((rows, cols), bf16),

time: 47.6 us -> 48.8 us (1.025)
  Pallas kernels: 45.7 us -> 46.9 us
    pallas_call x1, Pallas kernels: 45.7 us -> 46.9 us  [fused(): pl.pallas_call(functools.partial(fused_kernel, nz, ny), out_shape=jax.Sha...]
where the time goes in v2:
time: 48.8 us; the launch traced here: 48.6 us
  Pallas kernels  46.9 us (96%)
  local copies, waits for them, and re-layouts  1.77 us (4%)
    pallas_call x1, Pallas kernels, fused(): pl.pallas_call(functools.partial(fused_kernel, nz, ny), out_shape=jax.Sha...  46.9 us
    unnamed x1, local copies, waits for them, and re-layouts  1.77 us

profile of v2, /device:TPU:0, one launch (start us, length us, event | category | flops | bytes accessed | tf_op | source)
XLA Modules:
  0.0 48.6 jit_solution(1700633189034411870)
XLA Ops:
  0.0 46.9 %shard_map.82 = bf16[384,512]{1,0:T(8,128)(2,1)} custom-call(bf16[384,512]{1,0:T(8,128)(2,1)} %tok.1, bf16[1024,256]{1,0:T(8,128)(2,1)} %wq.1, bf16[1024,256]{1,0:T(8,128)(2,1)} %wk.1, bf16[1024,256]{1,0:T(8,128)(2,1)} %wv.1, bf16[256,1024]{1,0:T(8,128)(2,1)} %wo.1, f32[1,256]{1,0:T(1,128)} %bitcast.1, s32[6,8]{1,0:T(8,128)} %owner.1, s32[6,8]{1,0:T(8,128)} %local.1), custom_call_target="tpu_custom_call" | custom-call | tf_op jit(solution)/shard_map/pallas_call | solution.py:495
  46.9 1.8 %copy.10 = bf16[384,512]{1,0:T(8,128)(2,1)} copy(bf16[384,512]{1,0:T(8,128)(2,1)} %shard_map.82) | data formatting | bytes 786432
